TPU v7x, 512 devices: a whole 4x8x8 slice. The times are simulated.
512 devices in a mesh: sp: 64 (over z, y), tp: 8 (over x, core).
Axes of the slice: x: 4, y: 8, z: 8, core: 2. Of those that a mesh axis runs over, the one named last changes fastest.
Arguments:
- tokens: bfloat16 [65536, 2048], P(('sp', 'tp')), may hold values from -6 to 6
- norm_gain: float32 [2048], replicated, may hold values from 0.1 to 1.9
- w_query: bfloat16 [2048, 2048], P('sp', 'tp'), may hold values from -0.125 to 0.125
- w_key: bfloat16 [2048, 2048], P('sp', 'tp'), may hold values from -0.125 to 0.125
- w_value: bfloat16 [2048, 4096], P('sp', 'tp'), may hold values from -0.125 to 0.125
- w_rank_down: bfloat16 [2048, 16], replicated, may hold values from -0.125 to 0.125
- w_rank_up: bfloat16 [16, 2048], P(None, 'tp'), may hold values from -1.5 to 1.5
- gate_bias: float32 [2048], P('tp')
- decay_shift: float32 [65536], P('sp'), may hold values from -1 to 0
- out_gain: float32 [512], replicated, may hold values from 0.1 to 1.9
- w_out: bfloat16 [4096, 2048], P('tp', 'sp'), may hold values from -0.09375 to 0.09375
Outputs:
- mixed: bfloat16 [65536, 2048], P(('sp', 'tp'))
All inputs are finite; a program needn't handle non-finite values.
Results may differ from a plain program's by a relative error of at most 0.015.
Values may be sent and summed in bfloat16 or wider, within the bound.
A program may use at most 128 MiB of HBM per device.

v0:
```python
import jax
import jax.numpy as jnp
from jax import lax
from jax.sharding import Mesh
from jax.sharding import PartitionSpec as P

DK = 256
DV = 512
TAU = 16
BLOCK = 64
SP = ("sp_0", "sp_1")
SP_TP = ("sp_0", "sp_1", "tp")
EPS = 1e-06


def sent_together(arrays, axis, dim, along):
    both = jnp.concatenate(arrays, axis=along)
    out, at, finished = (lax.all_gather(both, axis, axis=dim, tiled=True), 0, [])
    for a in arrays:
        finished.append(lax.slice_in_dim(out, at, at + a.shape[along], axis=along))
        at += a.shape[along]
    return tuple(finished)


def filled_with(value, identity):
    return jax.tree.map(
        lambda a, e: jnp.broadcast_to(jnp.asarray(e, a.dtype), a.shape), value, identity
    )


def entering(value, axes, combine, identity):
    before = start = filled_with(value, identity)
    total = value
    for axis in reversed(axes):
        size, mine = (lax.axis_size(axis), lax.axis_index(axis))
        pieces = jax.tree.map(lambda part: lax.all_gather(part, axis), total)
        inside, total = (start, start)
        for k in range(size):
            passed = k < mine
            total = combine(total, jax.tree.map(lambda part: part[k], pieces))
            inside = jax.tree.map(lambda new, old: jnp.where(passed, new, old), total, inside)
        before = combine(inside, before)
    return before


def cut_along(value, dim, size):
    before, after = (value.shape[:dim], value.shape[dim + 1 :])
    return jnp.moveaxis(value.reshape(*before, size, -1, *after), dim, 0)


def sent_and_summed(value, axis, dim):
    size = lax.axis_size(axis)
    parts = lax.all_to_all(cut_along(value, dim, size), axis, 0, 0, tiled=True)
    return jnp.sum(parts.astype(jnp.float32), axis=0)


def rms_rows(values, gain):
    wide = values.astype(jnp.float32)
    return wide * lax.rsqrt(jnp.mean(wide * wide, axis=-1, keepdims=True) + EPS) * gain


def local_pass(query, key, value, log_decay, state):
    rows, heads, width = query.shape
    blocks = rows // BLOCK

    def split(tensor):
        return tensor.reshape((blocks, BLOCK) + tensor.shape[1:])

    causal = jnp.tril(jnp.ones((BLOCK, BLOCK), dtype=bool))

    def local_step(carry, inputs):
        q_blk, k_blk, v_blk, g_blk = inputs
        cumul = jnp.cumsum(g_blk, axis=0)
        centre = cumul - cumul[BLOCK // 2]
        q_scaled = (q_blk * jnp.exp(centre)).astype(jnp.bfloat16)
        k_scaled = (k_blk * jnp.exp(-centre)).astype(jnp.bfloat16)
        scores = jnp.einsum("ihd,jhd->hij", q_scaled, k_scaled, preferred_element_type=jnp.float32)
        scores = jnp.where(causal[None], scores, 0.0).astype(jnp.bfloat16)
        within = jnp.einsum("hij,jhe->ihe", scores, v_blk, preferred_element_type=jnp.float32)
        final = cumul[-1]
        decayed = (k_blk * jnp.exp(final - cumul)).astype(jnp.bfloat16)
        nxt = jnp.exp(final)[:, :, None] * carry + jnp.einsum(
            "jhd,jhe->hde", decayed, v_blk, preferred_element_type=jnp.float32
        )
        return (nxt, (within, q_blk * jnp.exp(cumul), final, carry))

    carry, (within, reach, finals, starts) = lax.scan(
        local_step, state, (split(query), split(key), split(value), split(log_decay))
    )
    return (within, reach, finals, starts, carry)


def state_only(key, value, log_decay, state):
    rows, heads, width = key.shape
    blocks = rows // BLOCK

    def split(tensor):
        return tensor.reshape((blocks, BLOCK) + tensor.shape[1:])

    def state_step(carry, inputs):
        k_blk, v_blk, g_blk = inputs
        cumul = jnp.cumsum(g_blk, axis=0)
        final = cumul[-1]
        decayed = (k_blk * jnp.exp(final - cumul)).astype(jnp.bfloat16)
        carry = jnp.exp(final)[:, :, None] * carry + jnp.einsum(
            "jhd,jhe->hde", decayed, v_blk, preferred_element_type=jnp.float32
        )
        return (carry, final)

    carry, finals = lax.scan(state_step, state, (split(key), split(value), split(log_decay)))
    return (carry, finals)


def read_out(reach, starts):
    blocks, block, heads, width = reach.shape
    result = jnp.einsum(
        "nihd,nhde->nihe",
        reach.astype(jnp.bfloat16),
        starts.astype(jnp.bfloat16),
        preferred_element_type=jnp.float32,
    )
    return result.reshape(blocks * block, heads, -1)


def combine(earlier, later):
    return (earlier[0] * later[0], later[0][:, :, None] * earlier[1] + later[1])


def on_device(
    tokens,
    norm_gain,
    w_query,
    w_key,
    w_value,
    w_rank_down,
    w_rank_up,
    gate_bias,
    decay_shift,
    out_gain,
    w_out,
):
    normed = rms_rows(tokens, norm_gain).astype(jnp.bfloat16)
    query_w, key_w, value_w = sent_together((w_query, w_key, w_value), SP, 0, 1)
    keys_here = query_w.shape[1]
    vals_here = value_w.shape[1]
    heads_here = keys_here // DK
    w_joined = jnp.concatenate([query_w, key_w, value_w, w_rank_down], axis=1)
    joined = jnp.dot(
        lax.all_gather(normed, "tp", axis=0, tiled=True),
        w_joined,
        preferred_element_type=jnp.float32,
    ).astype(jnp.bfloat16)
    span = joined.shape[0]
    q_heads = joined[:, :keys_here].astype(jnp.float32).reshape(span, heads_here, DK) * DK ** (-0.5)
    k_heads = joined[:, keys_here : 2 * keys_here].astype(jnp.float32).reshape(span, heads_here, DK)
    v_heads = joined[:, 2 * keys_here : 2 * keys_here + vals_here].reshape(span, heads_here, DV)
    rank = joined[:, 2 * keys_here + vals_here :]
    pre = jnp.dot(rank, w_rank_up, preferred_element_type=jnp.float32) + gate_bias
    log_decay = (jax.nn.log_sigmoid(pre) / TAU + decay_shift[:, None]).reshape(span, heads_here, DK)
    empty = jnp.zeros((heads_here, DK, DV), jnp.float32)
    identity = (jnp.ones((heads_here, DK), jnp.float32), empty)
    local_end, finals = state_only(k_heads, v_heads, log_decay, empty)
    carried = entering((jnp.exp(jnp.sum(finals, axis=0)), local_end), SP, combine, identity)[1]
    within, reach, _, starts, _ = local_pass(q_heads, k_heads, v_heads, log_decay, carried)
    attended = within.reshape(span, heads_here, DV) + read_out(reach, starts)
    shaped = rms_rows(attended, out_gain).astype(jnp.bfloat16).reshape(span, heads_here * DV)
    out_whole = lax.all_gather(w_out, SP, axis=1, tiled=True)
    return sent_and_summed(
        jnp.dot(shaped, out_whole, preferred_element_type=jnp.float32).astype(jnp.bfloat16), "tp", 0
    ).astype(jnp.bfloat16)


def solution(mesh):
    finer = Mesh(mesh.devices.reshape(8, 8, mesh.shape["tp"]), ("sp_0", "sp_1", "tp"))
    in_specs = (
        P(SP_TP, None),
        P(),
        P(SP, "tp"),
        P(SP, "tp"),
        P(SP, "tp"),
        P(),
        P(None, "tp"),
        P("tp"),
        P(SP),
        P(),
        P("tp", SP),
    )
    out_specs = P(SP_TP, None)
    return jax.shard_map(
        on_device, mesh=finer, in_specs=in_specs, out_specs=out_specs, check_vma=False
    )
```

profile of v0, /device:TPU:1, one launch (start us, length us, event | category | flops | bytes accessed | tf_op | source)
XLA Modules:
  0.0 498.0 jit_solution(9612616746641343713)
XLA Ops:
  7.8 2.0 fusion.61
  12.5 40.7 %all-gather.9.cloned.1.call-done = bf16[1024,2048]{1,0:T(8,128)(2,1)} async-done(((bf16[128,2048]{1,0:T(8,128)(2,1)}), bf16[1024,2048]{1,0:T(8,128)(2,1)}) %all-gather.9.cloned.1.call-update) | async-done | bytes 4194320 | tf_op jit(solution)/shard_map/all_gather | solution.py:149
  53.2 85.4 %all-gather.11.cloned.1.call-done = bf16[2048,1024]{1,0:T(8,128)(2,1)} async-done(((bf16[32,1024]{1,0:T(8,128)(2,1)}), bf16[2048,1024]{1,0:T(8,128)(2,1)}) %all-gather.11.cloned.1.call-update) | async-done | bytes 4194320 | tf_op jit(solution)/shard_map/all_gather | solution.py:18
  138.6 8.1 %fusion.51 = bf16[1024,1040]{0,1:T(8,128)(2,1)S(1)} fusion(bf16[1024,2048]{1,0:T(8,128)(2,1)} %all-gather.9.cloned.1.call-done, bf16[2048,16]{1,0:T(8,128)(2,1)S(1)} %copy.37, bf16[2048,1024]{1,0:T(8,128)(2,1)} %all-gather.11.cloned.1.call-done), kind=kOutput, calls=%fused_computation.62 | convolution fusion | flops 4371660800 | bytes 10584064 | tf_op jit(solution)/shard_map/dot_general | solution.py:148
  148.0 1.9 fusion.64
  149.8 2.5 copy.39
  152.4 3.4 copy.42
  157.3 2.1 copy.43
  160.7 48.5 %while.31 = (s32[]{:T(128)}, f32[1,256,512]{2,1,0:T(8,128)S(1)}, f32[16,1,256]{2,1,0:T(1,128)S(1)}, f32[16,64,1,256]{3,2,1,0:T(1,128)}, f32[16,64,1,256]{3,2,1,0...) while((s32[]{:T(128)}, f32[1,256,512]{2,1,0:T(8,128)S(1)}, ...), condition=%wide.region_3.4_spmd.clone, body=%wide.region_1.3_spmd.clone.sunk | while | flops 18251780 | bytes 1450087 | solution.py:110
  210.2 11.0 %all-gather.2 = f32[8,1,256]{2,1,0:T(1,128)S(1)} all-gather(f32[1,1,256]{2,1,0:T(1,128)S(1)} %bitcast.299), channel_id=2, replica_groups=mesh['sp_0'=8,'sp_1'=8,'tp'=8] {'sp_1'}, dimensions={0}, use_global_device_ids=true | all-gather | bytes 9216 | tf_op jit(solution)/shard_map/all_gather | solution.py:36
  221.2 46.4 %all-gather.17.cloned.1.call-done = f32[8,256,512]{2,1,0:T(8,128)} async-done(((f32[1,256,512]{2,1,0:T(8,128)}), f32[8,256,512]{2,1,0:T(8,128)}) %all-gather.17.cloned.1.call-update) | async-done | bytes 4194320 | tf_op jit(solution)/shard_map/all_gather | solution.py:36
  267.6 3.3 bitcast_add_fusion.1
  271.7 13.7 %all_gather.30 = f32[8,1,256]{2,1,0:T(1,128)S(1)} all-gather(f32[1,1,256]{2,1,0:T(1,128)S(1)} %get-tuple-element.230), channel_id=1, replica_groups=mesh['sp_0'=8,'sp_1'=8,'tp'=8] {'sp_0'}, dimensions={0}, use_global_device_ids=true | all-gather | bytes 9216 | tf_op jit(solution)/shard_map/all_gather | solution.py:36
  285.7 42.6 %all-gather.13.cloned.1.call-done = f32[8,1,256,512]{3,2,1,0:T(8,128)} async-done(((f32[1,1,256,512]{3,2,1,0:T(8,128)}), f32[8,1,256,512]{3,2,1,0:T(8,128)}) %all-gather.13.cloned.1.call-update) | async-done | bytes 4194320 | tf_op jit(solution)/shard_map/all_gather | solution.py:36
  328.3 4.3 fusion.68
  332.6 93.2 %while.30 = (s32[]{:T(128)}, f32[1,256,512]{2,1,0:T(8,128)S(1)}, f32[16,64,1,512]{3,1,2,0:T(8,128)}, bf16[16,64,1,256]{3,1,0,2:T(8,128)(2,1)S(1)}, bf16[16,1,256...) while((s32[]{:T(128)}, f32[1,256,512]{2,1,0:T(8,128)S(1)}, ...), condition=%wide.region_7.8_spmd.clone, body=%wide.region_5.7_spmd.clone.sunk | while | flops 24555520 | bytes 3223153 | solution.py:87
  334.8 1.8 fusion.117
  340.6 1.8 fusion.117
  346.4 1.8 fusion.117
  358.0 1.8 fusion.117
  363.9 1.8 fusion.117
  369.7 1.8 fusion.117
  375.5 1.8 fusion.117
  381.4 1.8 fusion.117
  393.0 1.8 fusion.117
  404.7 1.8 fusion.117
  410.5 1.8 fusion.117
  416.3 1.8 fusion.117
  425.8 3.8 multiply_reduce_fusion
  430.0 4.0 convolution_convert_fusion
  434.0 53.6 %all_to_all.5 = bf16[8,128,2048]{2,1,0:T(8,128)(2,1)} all-to-all(bf16[8,128,2048]{2,1,0:T(8,128)(2,1)S(1)} %bitcast.263), channel_id=1, replica_groups=mesh['sp_0'=8,'sp_1'=8,'tp'=8] {'tp'}, dimensions={0} | all-to-all | bytes 8388608 | tf_op jit(solution)/shard_map/all_to_all | solution.py:53
  487.7 3.8 reduce_sum.42
  (265 shorter events, 129.1 us)
Async XLA Ops:
  6.5 141.4 %copy-start = (bf16[16,256]{1,0:T(8,128)(2,1)S(1)}, bf16[16,256]{1,0:T(8,128)(2,1)}, u32[]{:S(2)}) copy-start(bf16[16,256]{1,0:T(8,128)(2,1)} %param.21) | copy-start | bytes 24580
  6.5 46.7 %all-gather.9.cloned.1.call-start = ((), (), s32[]{:S(2)}) async-start(), calls=%async_computation.1 | async-start | bytes 4718592 | tf_op jit(solution)/shard_map/all_gather | solution.py:149
  9.8 128.8 %all-gather.11.cloned.1.call-start = ((), (), s32[]{:S(2)}) async-start(), calls=%async_computation.2 | async-start | bytes 4259840 | tf_op jit(solution)/shard_map/all_gather | solution.py:18
  11.3 256.3 %all-gather.17.cloned.1.call-start = ((), (), s32[]{:S(2)}) async-start(), calls=%async_computation.5 | async-start | bytes 4718592 | tf_op jit(solution)/shard_map/all_gather | solution.py:36
  12.5 135.5 %copy-start.6 = (f32[1024]{0:T(1024)S(1)}, f32[1024]{0:T(1024)}, u32[]{:S(2)}) copy-start(f32[1024]{0:T(1024)} %param.23) | copy-start | bytes 12292
  12.5 135.4 %copy-start.7 = (f32[256]{0:T(256)S(1)}, f32[256]{0:T(256)}, u32[]{:S(2)}) copy-start(f32[256]{0:T(256)} %param.22) | copy-start | bytes 3076
  146.7 5.6 %copy-start.2 = (bf16[1024,1040]{0,1:T(8,128)(2,1)}, bf16[1024,1040]{0,1:T(8,128)(2,1)S(1)}, u32[]{:S(2)}) copy-start(bf16[1024,1040]{0,1:T(8,128)(2,1)S(1)} %fusion.51) | copy-start | bytes 6389764
  152.4 7.1 %slice-start = ((bf16[1024,1040]{0,1:T(8,128)(2,1)}), bf16[1024,512]{0,1:T(8,128)(2,1)S(1)}, s32[]{:S(2)}) async-start(bf16[1024,1040]{0,1:T(8,128)(2,1)} %copy-done.2), calls=%async_computation.6 | async-start | bytes 2097152 | tf_op jit(solution)/shard_map/slice | solution.py:156
  209.2 0.8 copy-start.1
  209.2 62.3 %copy-start.3 = (bf16[1024,1040]{0,1:T(8,128)(2,1)S(1)}, bf16[1024,1040]{0,1:T(8,128)(2,1)}, u32[]{:S(2)}) copy-start(bf16[1024,1040]{0,1:T(8,128)(2,1)} %copy-done.2) | copy-start | bytes 6389764
  210.0 118.2 %all-gather.13.cloned.1.call-start = ((), (), s32[]{:S(2)}) async-start(), calls=%async_computation.3 | async-start | bytes 4718592 | tf_op jit(solution)/shard_map/all_gather | solution.py:36
  270.9 159.1 %all-gather.15.cloned.1.call-start = ((), (), s32[]{:S(2)}) async-start(), calls=%async_computation.4 | async-start | bytes 2129920 | tf_op jit(solution)/shard_map/all_gather | solution.py:167
  328.3 4.3 copy-start.4
  425.8 3.9 copy-start.5
Sparse Core Ops, SparseCore 0:
  10.0 43.2 all-gather.8
  56.3 82.2 all-gather.10
  210.2 57.3 all-gather.16
  271.0 57.2 all-gather.12
  331.2 77.5 all-gather.14
where the time goes:
time: 504 us; the launch traced here: 498 us
  waiting for transfers between devices  216 us (43%)
  matrix products  82.2 us (16%)
  other arithmetic  81 us (16%)
  blocking collectives  78.3 us (16%)
  local copies, waits for them, and re-layouts  25.8 us (5%)
  between operations  13.4 us (3%)
    all_gather x2, waiting for transfers between devices, entering(): pieces = jax.tree.map(lambda part: lax.all_gather(part, axis), total)  89 us
    all_gather x1, waiting for transfers between devices, sent_together(): lax.all_gather(both, axis, axis=dim, tiled=True)  85.4 us
    all_to_all x1, blocking collectives, sent_and_summed(): parts = lax.all_to_all(cut_along(value, dim, size), axis, 0, 0, tiled=True)  53.6 us
    all_gather x1, waiting for transfers between devices, on_device(): lax.all_gather(normed, 'tp', axis=0, tiled=True)  40.7 us
    dot_general x16, matrix products, local_step(): jnp.einsum('hij,jhe->ihe', scores, v_blk, preferred_element_type=jnp.floa...  28.5 us
    all_gather x2, blocking collectives, entering(): pieces = jax.tree.map(lambda part: lax.all_gather(part, axis), total)  24.7 us
    dot_general x16, matrix products, local_step(): jnp.einsum('jhd,jhe->hde', decayed, v_blk, preferred_element_type=jnp.flo...  18.3 us
    dot_general x16, matrix products, state_step(): jnp.einsum('jhd,jhe->hde', decayed, v_blk, preferred_element_type=jnp.flo...  17.7 us
  transfers between devices with their start and end apart: 5, of which 4 were waited for; matrix products, arithmetic and copies ran while one was open for 21% of the time, Pallas kernels for 0%

commit v1 on v0

--- a/solution.py
+++ b/solution.py
@@ -1,3 +1,4 @@
+import functools
 import jax
 import jax.numpy as jnp
 from jax import lax
@@ -11,6 +12,16 @@
 SP = ("sp_0", "sp_1")
 SP_TP = ("sp_0", "sp_1", "tp")
 EPS = 1e-06
+
+
+def point_positions(in_array, array_axis):
+    reached = jnp.stack([in_array] * lax.axis_size("tp"))
+    high = lax.all_to_all(reached, "tp", split_axis=0, concat_axis=0)
+    tmp = jnp.concatenate(high, array_axis)
+    return tmp
+
+
+link_samples_all = functools.partial(point_positions, array_axis=0)
 
 
 def sent_together(arrays, axis, dim, along):
@@ -145,11 +156,9 @@
     vals_here = value_w.shape[1]
     heads_here = keys_here // DK
     w_joined = jnp.concatenate([query_w, key_w, value_w, w_rank_down], axis=1)
-    joined = jnp.dot(
-        lax.all_gather(normed, "tp", axis=0, tiled=True),
-        w_joined,
-        preferred_element_type=jnp.float32,
-    ).astype(jnp.bfloat16)
+    joined = jnp.dot(link_samples_all(normed), w_joined, preferred_element_type=jnp.float32).astype(
+        jnp.bfloat16
+    )
     span = joined.shape[0]
     q_heads = joined[:, :keys_here].astype(jnp.float32).reshape(span, heads_here, DK) * DK ** (-0.5)
     k_heads = joined[:, keys_here : 2 * keys_here].astype(jnp.float32).reshape(span, heads_here, DK)

time: 504 us -> 464 us (0.921)
  waiting for transfers between devices: 216 us -> 164 us
  starting transfers between devices: 0.17 us -> 11.5 us
    all_gather x1, waiting for transfers between devices: 85.4 us -> 25.4 us  [sent_together(): lax.all_gather(both, axis, axis=dim, tiled=True)]
    all_to_all x0 -> x1, waiting for transfers between devices: none -> 48.5 us  [point_positions(): high = lax.all_to_all(reached, 'tp', split_axis=0, concat_axis=0)]
    all_gather x1 -> x0, waiting for transfers between devices: 40.7 us -> none  [on_device(): lax.all_gather(normed, 'tp', axis=0, tiled=True)]
    all_to_all x0 -> x1, starting transfers between devices: none -> 11.4 us  [point_positions(): high = lax.all_to_all(reached, 'tp', split_axis=0, concat_axis=0)]
  transfers between devices with their start and end apart: 5 -> 5, of which waited for: 4 -> 4; matrix products, arithmetic and copies ran while one was open for 21% -> 23% of each run, Pallas kernels for 0% -> 0%
where the time goes in v1:
time: 464 us; the launch traced here: 458 us
  waiting for transfers between devices  164 us (35%)
  matrix products  82.2 us (18%)
  other arithmetic  80.2 us (17%)
  blocking collectives  78.3 us (17%)
  local copies, waits for them, and re-layouts  27.5 us (6%)
  between operations  13.4 us (3%)
  starting transfers between devices  11.5 us (2%)
    all_gather x2, waiting for transfers between devices, entering(): pieces = jax.tree.map(lambda part: lax.all_gather(part, axis), total)  89 us
    all_to_all x1, blocking collectives, sent_and_summed(): parts = lax.all_to_all(cut_along(value, dim, size), axis, 0, 0, tiled=True)  53.6 us
    all_to_all x1, waiting for transfers between devices, point_positions(): high = lax.all_to_all(reached, 'tp', split_axis=0, concat_axis=0)  48.5 us
    dot_general x16, matrix products, local_step(): jnp.einsum('hij,jhe->ihe', scores, v_blk, preferred_element_type=jnp.floa...  28.5 us
    all_gather x1, waiting for transfers between devices, sent_together(): lax.all_gather(both, axis, axis=dim, tiled=True)  25.4 us
    all_gather x2, blocking collectives, entering(): pieces = jax.tree.map(lambda part: lax.all_gather(part, axis), total)  24.7 us
    dot_general x16, matrix products, local_step(): jnp.einsum('jhd,jhe->hde', decayed, v_blk, preferred_element_type=jnp.flo...  18.3 us
    dot_general x16, matrix products, state_step(): jnp.einsum('jhd,jhe->hde', decayed, v_blk, preferred_element_type=jnp.flo...  17.7 us
  transfers between devices with their start and end apart: 5, of which 4 were waited for; matrix products, arithmetic and copies ran while one was open for 23% of the time, Pallas kernels for 0%

profile of v1, /device:TPU:1, one launch (start us, length us, event | category | flops | bytes accessed | tf_op | source)
XLA Modules:
  0.0 458.0 jit_solution(4430962109284820241)
XLA Ops:
  10.4 2.5 stack.2
  12.9 11.4 %all-to-all-start = ((bf16[8,128,2048]{2,1,0:T(8,128)(2,1)}), bf16[8,128,2048]{2,1,0:T(8,128)(2,1)}, u32[]{:S(2)}, u32[]{:S(2)}) async-start(bf16[8,128,2048]{2,1,0:T(8,128)(2,1)} %stack.2), calls=%async_computation | async-start | bytes 8388608 | tf_op jit(solution)/shard_map/all_to_all | solution.py:19
  24.6 48.5 %all-to-all-done = bf16[8,128,2048]{2,1,0:T(8,128)(2,1)} async-done(((bf16[8,128,2048]{2,1,0:T(8,128)(2,1)}), bf16[8,128,2048]{2,1,0:T(8,128)(2,1)}, u32[]{:S(2)}, u32[]{:S(2)}) %all-to-all-start) | async-done | bytes 4194336 | tf_op jit(solution)/shard_map/all_to_all | solution.py:19
  73.2 25.4 %all-gather.8.cloned.1.call-done = bf16[2048,1024]{1,0:T(8,128)(2,1)} async-done(((bf16[32,1024]{1,0:T(8,128)(2,1)}), bf16[2048,1024]{1,0:T(8,128)(2,1)}) %all-gather.8.cloned.1.call-update) | async-done | bytes 4194320 | tf_op jit(solution)/shard_map/all_gather | solution.py:29
  98.6 8.1 %fusion.51 = bf16[1024,1040]{0,1:T(8,128)(2,1)S(1)} fusion(bf16[1024,2048]{1,0:T(8,128)(2,1)} %bitcast, bf16[2048,16]{1,0:T(8,128)(2,1)S(1)} %copy.37, bf16[2048,1024]{1,0:T(8,128)(2,1)} %all-gather.8.cloned.1.call-done), kind=kOutput, calls=%fused_computation.62 | convolution fusion | flops 4371660800 | bytes 10584064 | tf_op jit(solution)/shard_map/dot_general | solution.py:159
  107.9 1.9 fusion.64
  109.8 2.5 copy.39
  112.3 3.4 copy.42
  117.3 2.1 copy.43
  120.7 48.5 %while.31 = (s32[]{:T(128)}, f32[1,256,512]{2,1,0:T(8,128)S(1)}, f32[16,1,256]{2,1,0:T(1,128)S(1)}, f32[16,64,1,256]{3,2,1,0:T(1,128)}, f32[16,64,1,256]{3,2,1,0...) while((s32[]{:T(128)}, f32[1,256,512]{2,1,0:T(8,128)S(1)}, ...), condition=%wide.region_3.4_spmd.clone, body=%wide.region_1.3_spmd.clone.sunk | while | flops 18251780 | bytes 1450087 | solution.py:121
  170.1 11.0 %all-gather.2 = f32[8,1,256]{2,1,0:T(1,128)S(1)} all-gather(f32[1,1,256]{2,1,0:T(1,128)S(1)} %bitcast.300), channel_id=2, replica_groups=mesh['sp_0'=8,'sp_1'=8,'tp'=8] {'sp_1'}, dimensions={0}, use_global_device_ids=true | all-gather | bytes 9216 | tf_op jit(solution)/shard_map/all_gather | solution.py:47
  181.2 46.4 %all-gather.14.cloned.1.call-done = f32[8,256,512]{2,1,0:T(8,128)} async-done(((f32[1,256,512]{2,1,0:T(8,128)}), f32[8,256,512]{2,1,0:T(8,128)}) %all-gather.14.cloned.1.call-update) | async-done | bytes 4194320 | tf_op jit(solution)/shard_map/all_gather | solution.py:47
  227.6 3.3 bitcast_add_fusion.1
  231.6 13.7 %all_gather.26 = f32[8,1,256]{2,1,0:T(1,128)S(1)} all-gather(f32[1,1,256]{2,1,0:T(1,128)S(1)} %get-tuple-element.230), channel_id=1, replica_groups=mesh['sp_0'=8,'sp_1'=8,'tp'=8] {'sp_0'}, dimensions={0}, use_global_device_ids=true | all-gather | bytes 9216 | tf_op jit(solution)/shard_map/all_gather | solution.py:47
  245.7 42.6 %all-gather.10.cloned.1.call-done = f32[8,1,256,512]{3,2,1,0:T(8,128)} async-done(((f32[1,1,256,512]{3,2,1,0:T(8,128)}), f32[8,1,256,512]{3,2,1,0:T(8,128)}) %all-gather.10.cloned.1.call-update) | async-done | bytes 4194320 | tf_op jit(solution)/shard_map/all_gather | solution.py:47
  288.3 4.3 fusion.68
  292.6 93.2 %while.30 = (s32[]{:T(128)}, f32[1,256,512]{2,1,0:T(8,128)S(1)}, f32[16,64,1,512]{3,1,2,0:T(8,128)}, bf16[16,64,1,256]{3,1,0,2:T(8,128)(2,1)S(1)}, bf16[16,1,256...) while((s32[]{:T(128)}, f32[1,256,512]{2,1,0:T(8,128)S(1)}, ...), condition=%wide.region_7.8_spmd.clone, body=%wide.region_5.7_spmd.clone.sunk | while | flops 24555520 | bytes 3223153 | solution.py:98
  294.7 1.8 fusion.117
  300.6 1.8 fusion.117
  306.4 1.8 fusion.117
  318.0 1.8 fusion.117
  323.9 1.8 fusion.117
  329.7 1.8 fusion.117
  335.5 1.8 fusion.117
  341.3 1.8 fusion.117
  353.0 1.8 fusion.117
  364.6 1.8 fusion.117
  376.3 1.8 fusion.117
  385.8 3.8 multiply_reduce_fusion
  390.0 4.0 convolution_convert_fusion
  394.0 53.6 %all_to_all.10 = bf16[8,128,2048]{2,1,0:T(8,128)(2,1)} all-to-all(bf16[8,128,2048]{2,1,0:T(8,128)(2,1)S(1)} %bitcast.264), channel_id=1, replica_groups=mesh['sp_0'=8,'sp_1'=8,'tp'=8] {'tp'}, dimensions={0} | all-to-all | bytes 8388608 | tf_op jit(solution)/shard_map/all_to_all | solution.py:64
  447.6 3.8 reduce_sum.42
  (267 shorter events, 131.2 us)
Async XLA Ops:
  6.5 101.4 %copy-start = (bf16[16,256]{1,0:T(8,128)(2,1)S(1)}, bf16[16,256]{1,0:T(8,128)(2,1)}, u32[]{:S(2)}) copy-start(bf16[16,256]{1,0:T(8,128)(2,1)} %param.21) | copy-start | bytes 24580
  6.5 92.0 %all-gather.8.cloned.1.call-start = ((), (), s32[]{:S(2)}) async-start(), calls=%async_computation.2 | async-start | bytes 4259840 | tf_op jit(solution)/shard_map/all_gather | solution.py:29
  12.9 11.4 %copy-start.5 = (bf16[2048,16]{0,1:T(8,128)(2,1)S(1)}, bf16[2048,16]{0,1:T(8,128)(2,1)}, u32[]{:S(2)}) copy-start(bf16[2048,16]{0,1:T(8,128)(2,1)} %param.20) | copy-start | bytes 196612
  12.9 60.2 %all-to-all-start = ((bf16[8,128,2048]{2,1,0:T(8,128)(2,1)}), bf16[8,128,2048]{2,1,0:T(8,128)(2,1)}, u32[]{:S(2)}, u32[]{:S(2)}) async-start(bf16[8,128,2048]{2,1,0:T(8,128)(2,1)} %stack.2), calls=%async_computation | async-start | bytes 8388608 | tf_op jit(solution)/shard_map/all_to_all | solution.py:19
  24.3 203.2 %all-gather.14.cloned.1.call-start = ((), (), s32[]{:S(2)}) async-start(), calls=%async_computation.5 | async-start | bytes 4718592 | tf_op jit(solution)/shard_map/all_gather | solution.py:47
  98.6 9.4 %copy-start.7 = (f32[1024]{0:T(1024)S(1)}, f32[1024]{0:T(1024)}, u32[]{:S(2)}) copy-start(f32[1024]{0:T(1024)} %param.23) | copy-start | bytes 12292
  98.6 9.4 %copy-start.8 = (f32[256]{0:T(256)S(1)}, f32[256]{0:T(256)}, u32[]{:S(2)}) copy-start(f32[256]{0:T(256)} %param.22) | copy-start | bytes 3076
  106.7 5.6 %copy-start.2 = (bf16[1024,1040]{0,1:T(8,128)(2,1)}, bf16[1024,1040]{0,1:T(8,128)(2,1)S(1)}, u32[]{:S(2)}) copy-start(bf16[1024,1040]{0,1:T(8,128)(2,1)S(1)} %fusion.51) | copy-start | bytes 6389764
  112.3 7.1 %slice-start = ((bf16[1024,1040]{0,1:T(8,128)(2,1)}), bf16[1024,512]{0,1:T(8,128)(2,1)S(1)}, s32[]{:S(2)}) async-start(bf16[1024,1040]{0,1:T(8,128)(2,1)} %copy-done.2), calls=%async_computation.6 | async-start | bytes 2097152 | tf_op jit(solution)/shard_map/slice | solution.py:165
  169.2 0.8 copy-start.1
  169.2 62.3 %copy-start.3 = (bf16[1024,1040]{0,1:T(8,128)(2,1)S(1)}, bf16[1024,1040]{0,1:T(8,128)(2,1)}, u32[]{:S(2)}) copy-start(bf16[1024,1040]{0,1:T(8,128)(2,1)} %copy-done.2) | copy-start | bytes 6389764
  170.0 118.2 %all-gather.10.cloned.1.call-start = ((), (), s32[]{:S(2)}) async-start(), calls=%async_computation.3 | async-start | bytes 4718592 | tf_op jit(solution)/shard_map/all_gather | solution.py:47
  230.9 159.1 %all-gather.12.cloned.1.call-start = ((), (), s32[]{:S(2)}) async-start(), calls=%async_computation.4 | async-start | bytes 2129920 | tf_op jit(solution)/shard_map/all_gather | solution.py:176
  288.3 4.3 copy-start.4
  385.8 3.9 copy-start.6
Sparse Core Ops, SparseCore 0:
  10.4 88.1 all-gather.7
  170.1 57.3 all-gather.13
  231.0 57.2 all-gather.9
  291.2 77.5 all-gather.11
